TPU v7x, 512 devices: a whole 4x4x16 slice. The times are simulated.
512 devices in a mesh: sp: 16 (over z), dp: 32 (over y, x, core).
Axes of the slice: x: 4, y: 4, z: 16, core: 2. Of those that a mesh axis runs over, the one named last changes fastest.
Arguments:
- cotangent: bfloat16 [32, 2048, 2048], P('dp', 'sp'), may hold values from -6 to 6
- unit_pre: bfloat16 [32, 2048, 2048], P('dp', None, 'sp'), may hold values from -6 to 6
- gate_pre: bfloat16 [32, 2048, 2048], P('dp', None, 'sp'), may hold values from -15 to 15
- out_weight: bfloat16 [2048, 2048], P('dp', 'sp'), may hold values from -0.125 to 0.125
- mix_weight: bfloat16 [8, 128, 128], replicated, may hold values from -0.5 to 0.5
- mix_bias: bfloat16 [8, 128], replicated, may hold values from 0.099609375 to 1.8984375
- norm_gain: bfloat16 [2048], P('sp'), may hold values from 0.099609375 to 1.8984375
- norm_shift: bfloat16 [2048], P('sp'), may hold values from -3 to 3
Outputs:
- unit_grad: bfloat16 [32, 2048, 2048], P('dp', None, 'sp')
- gate_grad: bfloat16 [32, 2048, 2048], P('dp', None, 'sp')
- out_weight_grad: float32 [2048, 2048], P('dp', 'sp')
- mix_weight_grad: float32 [8, 128, 128], replicated
- mix_bias_grad: float32 [8, 128], replicated
- gain_grad: float32 [2048], P('sp')
- shift_grad: float32 [2048], P('sp')
All inputs are finite; a program needn't handle non-finite values.
Results may differ from a plain program's by a relative error of at most 0.015.
Values may be sent and summed in bfloat16 or wider, within the bound.
A program may use at most 64 MiB of HBM per device.

v0:
```python
import math
import jax
import jax.numpy as jnp
from jax import lax
from jax.sharding import PartitionSpec as P

GW = 2048
GROUPS = 8
BLK = 128
epsilon = 1e-05
tanh_coef = math.sqrt(2.0 / math.pi)


def sum_over(x, axis):
    devices = lax.axis_size(axis)
    copies = jnp.broadcast_to(x[None], (devices, *x.shape))
    return lax.all_to_all(copies, axis, 0, 0, tiled=True).sum(axis=0)


def gelu_slope(values):
    inner = tanh_coef * (values + 0.044715 * values * values * values)
    hyper = jnp.tanh(inner)
    return 0.5 * (1.0 + hyper) + 0.5 * values * (1.0 - hyper * hyper) * tanh_coef * (
        1.0 + 3.0 * 0.044715 * values * values
    )


def local(cotangent, unit_pre, gate_pre, out_weight, mix_weight, mix_bias, norm_gain, norm_shift):
    seq_len = unit_pre.shape[1]
    channels = unit_pre.shape[2]
    group_dim = GW // GROUPS
    blocks = seq_len // BLK
    sp_size = lax.axis_size("sp")
    sp_at = lax.axis_index("sp")
    group = sp_at * channels // group_dim
    weight_rows = lax.all_gather(out_weight, "sp", axis=1, tiled=True)
    weight_whole = lax.all_gather(weight_rows, "dp", axis=0, tiled=True)
    units = unit_pre[0].astype(jnp.float32)
    gates = gate_pre[0].astype(jnp.float32)
    unit_act = jax.nn.gelu(units)
    gate_act = jax.nn.gelu(gates)
    moments = sum_over(
        jnp.stack([jnp.sum(gate_act, axis=-1), jnp.sum(gate_act * gate_act, axis=-1)]), "sp"
    )
    mean_val = moments[0] / GW
    var_val = moments[1] / GW - mean_val * mean_val
    rstd_val = lax.rsqrt(var_val + epsilon)
    centred = (gate_act - mean_val[:, None]) * rstd_val[:, None]
    gain_vec = norm_gain.astype(jnp.float32)
    normed = (centred * gain_vec + norm_shift.astype(jnp.float32)).astype(jnp.bfloat16)
    causal = jnp.arange(BLK)[:, None] >= jnp.arange(BLK)[None, :]
    local_weight = lax.dynamic_index_in_dim(mix_weight, group, 0, keepdims=False)
    masked = jnp.where(causal, local_weight, jnp.zeros_like(local_weight))
    local_bias = lax.dynamic_index_in_dim(mix_bias, group, 0, keepdims=False).astype(jnp.float32)
    normed_blocks = normed.reshape(blocks, BLK, channels)
    mixed = jnp.einsum("ts,nsd->ntd", masked, normed_blocks, preferred_element_type=jnp.float32)
    mixed = (mixed + local_bias[None, :, None]).reshape(seq_len, channels)
    gated = (unit_act * mixed).astype(jnp.bfloat16)
    gated_rows = lax.all_to_all(gated, "sp", split_axis=0, concat_axis=1, tiled=True)
    head_rows = jnp.dot(cotangent[0], weight_whole, preferred_element_type=jnp.float32)
    head = lax.all_to_all(
        head_rows.astype(jnp.bfloat16), "sp", split_axis=1, concat_axis=0, tiled=True
    ).astype(jnp.float32)
    weight_part = lax.dot_general(
        cotangent[0], gated_rows, (((0,), (0,)), ((), ())), preferred_element_type=jnp.float32
    ).astype(jnp.bfloat16)
    token_count = lax.axis_size("dp") * seq_len
    norm_scale = 1.0 / math.sqrt(token_count)
    mix_scale = 1.0 / math.sqrt(token_count // BLK * group_dim)
    plane_sum = lax.psum_scatter(weight_part, "dp", scatter_dimension=0, tiled=True)
    plane_parts = jnp.moveaxis(plane_sum.reshape(plane_sum.shape[0], sp_size, channels), 1, 0)
    arrived = lax.all_to_all(plane_parts, "sp", split_axis=0, concat_axis=0, tiled=True)
    out_grad = arrived.astype(jnp.float32).sum(axis=0) * norm_scale
    unit_grad = (head * mixed * gelu_slope(units)).astype(jnp.bfloat16)
    mix_grad = head * unit_act
    mix_round = mix_grad.astype(jnp.bfloat16).reshape(blocks, BLK, channels)
    mix_term = jnp.einsum(
        "ntd,nsd->ts", mix_round, normed_blocks, preferred_element_type=jnp.float32
    )
    mix_term = jnp.where(causal, mix_term, jnp.float32(0.0))
    bias_term = jnp.sum(mix_grad.reshape(blocks, BLK, channels), axis=(0, 2))
    normed_grad = jnp.einsum(
        "ts,ntd->nsd", masked, mix_round, preferred_element_type=jnp.float32
    ).reshape(seq_len, channels)
    gain_term = jnp.sum(normed_grad * centred, axis=0)
    shift_term = jnp.sum(normed_grad, axis=0)
    scaled = normed_grad * gain_vec
    back_sums = sum_over(
        jnp.stack([jnp.sum(scaled, axis=-1), jnp.sum(scaled * centred, axis=-1)]), "sp"
    )
    first_m = back_sums[0] / GW
    second_m = back_sums[1] / GW
    gate_grad = (
        rstd_val[:, None]
        * (scaled - first_m[:, None] - centred * second_m[:, None])
        * gelu_slope(gates)
    ).astype(jnp.bfloat16)
    group_hot = (jnp.arange(GROUPS) == group).astype(jnp.float32)
    own_hot = (jnp.arange(sp_size) == sp_at).astype(jnp.float32)
    packed = jnp.concatenate(
        [
            (group_hot[:, None, None] * mix_term).reshape(GROUPS * BLK, BLK),
            group_hot[:, None] * bias_term,
            own_hot[:, None] * gain_term,
            own_hot[:, None] * shift_term,
        ]
    )
    total = lax.psum(packed, ("sp", "dp"))
    top = GROUPS * BLK
    weight_total = total[:top].reshape(GROUPS, BLK, BLK)
    bias_total = total[top : top + GROUPS]
    tail = total[top + GROUPS :]
    gain_total = lax.dynamic_index_in_dim(tail, sp_at, 0, keepdims=False)
    shift_total = lax.dynamic_index_in_dim(tail, sp_size + sp_at, 0, keepdims=False)
    return (
        unit_grad[None],
        gate_grad[None],
        out_grad,
        weight_total * mix_scale,
        bias_total * mix_scale,
        gain_total * norm_scale,
        shift_total * norm_scale,
    )


def solution(mesh):
    return jax.shard_map(
        local,
        mesh=mesh,
        in_specs=(
            P("dp", "sp", None),
            P("dp", None, "sp"),
            P("dp", None, "sp"),
            P("dp", "sp"),
            P(),
            P(),
            P("sp"),
            P("sp"),
        ),
        out_specs=(
            P("dp", None, "sp"),
            P("dp", None, "sp"),
            P("dp", "sp"),
            P(),
            P(),
            P("sp"),
            P("sp"),
        ),
        check_vma=False,
    )
```

profile of v0, /device:TPU:32, one launch (start us, length us, event | category | flops | bytes accessed | tf_op | source)
XLA Modules:
  0.0 828.7 jit_solution(9951408123859522207)
XLA Ops:
  7.2 0.0 copy-start
  7.2 0.0 all-gather.2.cloned.1.call-start
  7.2 37.3 %all_gather.6 = bf16[64,2048]{1,0:T(8,128)(2,1)} all-gather(bf16[64,128]{1,0:T(8,128)(2,1)} %param.11), channel_id=1, replica_groups=mesh['sp'=16,'dp'=32] {'sp'}, dimensions={1}, use_global_device_ids=true | all-gather | bytes 278528 | tf_op jit(solution)/shard_map/all_gather | solution.py:36
  44.6 0.0 all-gather.2.cloned.1.call-update
  44.6 1.8 fusion.58
  46.4 0.8 broadcast_in_dim.11
  47.2 8.9 %all-to-all-start.1 = ((f32[16,2,2048]{2,1,0:T(2,128)}), f32[16,2,2048]{2,1,0:T(2,128)S(1)}, u32[]{:S(2)}, u32[]{:S(2)}) async-start(f32[16,2,2048]{2,1,0:T(2,128)} %broadcast_in_dim.11), calls=%async_computation.1 | async-start | bytes 524288 | tf_op jit(solution)/shard_map/all_to_all | solution.py:17
  56.1 0.0 copy-start.5
  56.1 0.0 copy-start.2
  56.1 0.0 copy-start.1
  56.1 54.5 %all-gather.2.cloned.1.call-done = bf16[2048,2048]{1,0:T(8,128)(2,1)} async-done(((bf16[64,2048]{1,0:T(8,128)(2,1)}), bf16[2048,2048]{1,0:T(8,128)(2,1)}) %all-gather.2.cloned.1.call-update) | async-done | bytes 8388624 | tf_op jit(solution)/shard_map/all_gather | solution.py:37
  110.6 0.0 copy-done
  110.6 4.6 fusion.5
  115.3 0.0 copy-start.6
  115.3 0.9 copy.53
  116.2 0.0 all-to-all-done.1
  116.2 12.7 %all-to-all-start = ((bf16[128,16,128]{2,0,1:T(8,128)(2,1)}), bf16[128,16,128]{2,0,1:T(8,128)(2,1)S(1)}, u32[]{:S(2)}, u32[]{:S(2)}) async-start(bf16[128,16,128]{2,0,1:T(8,128)(2,1)} %bitcast.135), calls=%async_computation | async-start | bytes 1048576 | tf_op jit(solution)/shard_map/all_to_all | solution.py:61
  128.9 0.0 copy-done.5
  128.9 0.1 reduce_sum.92
  129.0 29.5 %all-to-all-done = bf16[128,16,128]{2,0,1:T(8,128)(2,1)S(1)} async-done(((bf16[128,16,128]{2,0,1:T(8,128)(2,1)}), bf16[128,16,128]{2,0,1:T(8,128)(2,1)S(1)}, u32[]{:S(2)}, u32[]{:S(2)}) %all-to-all-start) | async-done | bytes 524320 | tf_op jit(solution)/shard_map/all_to_all | solution.py:61
  158.6 0.0 copy-done.2
  158.6 0.5 fusion.59
  159.1 0.0 copy-start.3
  159.1 1.0 copy-done.3
  160.1 0.0 copy-done.1
  160.1 3.3 fusion.56
  163.4 0.8 broadcast_in_dim.15
  164.2 6.1 all-to-all-start.2
  170.3 0.0 copy-done.6
  170.3 0.7 fusion.80
  171.0 17.5 %all-to-all-done.2 = f32[16,2,2048]{2,1,0:T(2,128)S(1)} async-done(((f32[16,2,2048]{2,1,0:T(2,128)}), f32[16,2,2048]{2,1,0:T(2,128)S(1)}, u32[]{:S(2)}, u32[]{:S(2)}) %all-to-all-start.2) | async-done | bytes 262176 | tf_op jit(solution)/shard_map/all_to_all | solution.py:17
  188.6 0.1 reduce_sum.95
  188.7 2.8 fusion.51
  191.5 3.0 multiply_convert_fusion
  194.4 6.1 all-to-all-start.3
  200.5 0.0 all-reduce.2.cloned.1.call-start
  200.6 0.3 reduce_sum.99
  200.8 0.1 broadcast_bitcast_fusion
  200.9 2.5 fusion.6
  203.5 0.2 bitcast_multiply_fusion.5
  203.7 0.1 broadcast_multiply_fusion.2
  203.7 0.8 pad_maximum_fusion
  204.6 0.0 all-reduce.2.cloned.1.call-update
  204.6 0.0 reduce-scatter.4.cloned.1.call-start
  204.6 24.2 %all-to-all-done.3 = bf16[16,128,128]{2,1,0:T(8,128)(2,1)S(1)} async-done(((bf16[16,128,128]{2,1,0:T(8,128)(2,1)}), bf16[16,128,128]{2,1,0:T(8,128)(2,1)S(1)}, u32[]{:S(2)}, u32[]{:S(2)}) %all-to-all-start.3) | async-done | bytes 524320 | tf_op jit(solution)/shard_map/all_to_all | solution.py:59
  228.9 0.3 copy.36
  229.2 5.5 convert_bitcast_fusion
  234.7 12.4 %copy.42 = bf16[2048,2048]{1,0:T(8,128)(2,1)} copy(bf16[2048,2048]{0,1:T(8,128)(2,1)} %convert_bitcast_fusion) | data formatting | bytes 16777216
  247.1 0.0 copy-start.4
  247.1 0.0 reduce-scatter.4.cloned.1.call-update
  247.1 423.4 %all-reduce.2.cloned.1.call-done = f32[1064,128]{1,0:T(8,128)} async-done(((f32[1064,128]{1,0:T(8,128)}), f32[1064,128]{1,0:T(8,128)}) %all-reduce.2.cloned.1.call-update) | async-done | bytes 544784 | tf_op jit(solution)/shard_map/psum | solution.py:108
  670.5 0.7 slice.34
  671.2 117.9 %reduce-scatter.4.cloned.1.call-done = bf16[64,2048]{1,0:T(8,128)(2,1)} async-done(((bf16[2048,2048]{1,0:T(8,128)(2,1)}), bf16[64,2048]{1,0:T(8,128)(2,1)}) %reduce-scatter.4.cloned.1.call-update) | async-done | bytes 262160
  789.1 1.2 copy.43
  790.4 0.9 copy.37
  791.3 12.7 %all-to-all-start.4 = ((bf16[16,64,128]{2,1,0:T(8,128)(2,1)}), bf16[16,64,128]{2,1,0:T(8,128)(2,1)S(1)}, u32[]{:S(2)}, u32[]{:S(2)}) async-start(bf16[16,64,128]{2,1,0:T(8,128)(2,1)} %bitcast.29), calls=%async_computation.4 | async-start | bytes 524288 | tf_op jit(solution)/shard_map/all_to_all | solution.py:72
  803.9 0.5 fusion.84
  804.5 1.3 slice_multiply_fusion.5
  805.7 1.9 slice_multiply_fusion
  807.6 0.0 copy-done.4
  807.6 1.5 fusion.30
  809.1 12.2 %all-to-all-done.4 = bf16[16,64,128]{2,1,0:T(8,128)(2,1)S(1)} async-done(((bf16[16,64,128]{2,1,0:T(8,128)(2,1)}), bf16[16,64,128]{2,1,0:T(8,128)(2,1)S(1)}, u32[]{:S(2)}, u32[]{:S(2)}) %all-to-all-start.4) | async-done | bytes 262176 | tf_op jit(solution)/shard_map/all_to_all | solution.py:72
  821.3 0.1 copy.46
  821.4 0.7 copy.39
  (12 shorter events, 0.1 us)
Async XLA Ops:
  7.2 103.5 %copy-start = (bf16[1,128,2048]{2,1,0:T(8,128)(2,1)S(1)}, bf16[1,128,2048]{2,1,0:T(8,128)(2,1)}, u32[]{:S(2)}) copy-start(bf16[1,128,2048]{2,1,0:T(8,128)(2,1)} %param.8) | copy-start | bytes 1572868
  7.2 103.4 %all-gather.2.cloned.1.call-start = ((), (), s32[]{:S(2)}) async-start(), calls=%async_computation.6 | async-start | bytes 8650752 | tf_op jit(solution)/shard_map/all_gather | solution.py:37
  47.2 69.0 %all-to-all-start.1 = ((f32[16,2,2048]{2,1,0:T(2,128)}), f32[16,2,2048]{2,1,0:T(2,128)S(1)}, u32[]{:S(2)}, u32[]{:S(2)}) async-start(f32[16,2,2048]{2,1,0:T(2,128)} %broadcast_in_dim.11), calls=%async_computation.1 | async-start | bytes 524288 | tf_op jit(solution)/shard_map/all_to_all | solution.py:17
  56.1 72.8 %copy-start.5 = (bf16[128]{0:T(256)(128)(2,1)S(1)}, bf16[128]{0:T(256)(128)(2,1)}, u32[]{:S(2)}) copy-start(bf16[128]{0:T(256)(128)(2,1)} %param.14) | copy-start | bytes 772
  56.1 102.5 %copy-start.2 = (bf16[1,2048,128]{2,1,0:T(8,128)(2,1)S(1)}, bf16[1,2048,128]{2,1,0:T(8,128)(2,1)}, u32[]{:S(2)}) copy-start(bf16[1,2048,128]{2,1,0:T(8,128)(2,1)} %param.9) | copy-start | bytes 1572868
  56.1 104.0 %copy-start.1 = (bf16[1,2048,128]{2,1,0:T(8,128)(2,1)S(1)}, bf16[1,2048,128]{2,1,0:T(8,128)(2,1)}, u32[]{:S(2)}) copy-start(bf16[1,2048,128]{2,1,0:T(8,128)(2,1)} %param.10) | copy-start | bytes 1572868
  115.3 55.1 %copy-start.6 = (bf16[128]{0:T(256)(128)(2,1)S(1)}, bf16[128]{0:T(256)(128)(2,1)}, u32[]{:S(2)}) copy-start(bf16[128]{0:T(256)(128)(2,1)} %param.15) | copy-start | bytes 772
  116.2 42.4 %all-to-all-start = ((bf16[128,16,128]{2,0,1:T(8,128)(2,1)}), bf16[128,16,128]{2,0,1:T(8,128)(2,1)S(1)}, u32[]{:S(2)}, u32[]{:S(2)}) async-start(bf16[128,16,128]{2,0,1:T(8,128)(2,1)} %bitcast.135), calls=%async_computation | async-start | bytes 1048576 | tf_op jit(solution)/shard_map/all_to_all | solution.py:61
  159.1 1.0 copy-start.3
  164.2 24.4 %all-to-all-start.2 = ((f32[16,2,2048]{2,1,0:T(2,128)}), f32[16,2,2048]{2,1,0:T(2,128)S(1)}, u32[]{:S(2)}, u32[]{:S(2)}) async-start(f32[16,2,2048]{2,1,0:T(2,128)} %broadcast_in_dim.15), calls=%async_computation.2 | async-start | bytes 524288 | tf_op jit(solution)/shard_map/all_to_all | solution.py:17
  194.4 34.5 %all-to-all-start.3 = ((bf16[16,128,128]{2,1,0:T(8,128)(2,1)}), bf16[16,128,128]{2,1,0:T(8,128)(2,1)S(1)}, u32[]{:S(2)}, u32[]{:S(2)}) async-start(bf16[16,128,128]{2,1,0:T(8,128)(2,1)} %get-tuple-element.36), calls=%async_computation.3 | async-start | bytes 1048576 | tf_op jit(solution)/shard_map/all_to_all | solution.py:59
  200.5 470.0 %all-reduce.2.cloned.1.call-start = ((), (), s32[]{:S(2)}) async-start(), calls=%async_computation.7 | async-start | bytes 1089536 | tf_op jit(solution)/shard_map/psum | solution.py:108
  204.6 584.5 %reduce-scatter.4.cloned.1.call-start = ((), (), s32[]{:S(2)}) async-start(), calls=%async_computation.8 | async-start | bytes 8650752
  247.1 560.5 %copy-start.4 = (f32[16,128,128]{2,1,0:T(8,128)S(1)}, f32[16,128,128]{2,1,0:T(8,128)}, u32[]{:S(2)}) copy-start(f32[16,128,128]{2,1,0:T(8,128)} %get-tuple-element.37) | copy-start | bytes 3145732
  791.3 30.0 %all-to-all-start.4 = ((bf16[16,64,128]{2,1,0:T(8,128)(2,1)}), bf16[16,64,128]{2,1,0:T(8,128)(2,1)S(1)}, u32[]{:S(2)}, u32[]{:S(2)}) async-start(bf16[16,64,128]{2,1,0:T(8,128)(2,1)} %bitcast.29), calls=%async_computation.4 | async-start | bytes 524288 | tf_op jit(solution)/shard_map/all_to_all | solution.py:72
Sparse Core Ops, SparseCore 0:
  44.7 65.8 all-gather.1
  206.8 463.6 all-reduce.1
  675.1 114.0 reduce-scatter.3
where the time goes:
time: 830 us; the launch traced here: 829 us
  waiting for transfers between devices  679 us (82%)
  starting transfers between devices  46.6 us (6%)
  blocking collectives  37.3 us (4%)
  local copies, waits for them, and re-layouts  19.8 us (2%)
  matrix products  18.9 us (2%)
  between operations  13.9 us (2%)
  other arithmetic  12.7 us (2%)
    psum x1, waiting for transfers between devices, local(): total = lax.psum(packed, ('sp', 'dp'))  423 us
    unnamed x4, waiting for transfers between devices  118 us
    all_gather x1, waiting for transfers between devices, local(): weight_whole = lax.all_gather(weight_rows, 'dp', axis=0, tiled=True)  54.5 us
    all_gather x1, blocking collectives, local(): weight_rows = lax.all_gather(out_weight, 'sp', axis=1, tiled=True)  37.3 us
    all_to_all x1, waiting for transfers between devices, local(): lax.all_to_all(head_rows.astype(jnp.bfloat16), 'sp', split_axis=1, concat...  29.5 us
    all_to_all x1, waiting for transfers between devices, local(): lax.all_to_all(gated, 'sp', split_axis=0, concat_axis=1, tiled=True)  24.2 us
    all_to_all x2, waiting for transfers between devices, sum_over(): return lax.all_to_all(copies, axis, 0, 0, tiled=True).sum(axis=0)  17.5 us
  transfers between devices with their start and end apart: 8, of which 7 were waited for; matrix products, arithmetic and copies ran while one was open for 4% of the time, Pallas kernels for 0%

commit v1 on v0

--- a/solution.py
+++ b/solution.py
@@ -105,7 +105,7 @@
             own_hot[:, None] * shift_term,
         ]
     )
-    total = lax.psum(packed, ("sp", "dp"))
+    total = lax.psum(lax.psum(packed, "sp"), "dp")
     top = GROUPS * BLK
     weight_total = total[:top].reshape(GROUPS, BLK, BLK)
     bias_total = total[top : top + GROUPS]

time: 830 us -> 635 us (0.77)
  waiting for transfers between devices: 679 us -> 485 us
    psum x1 -> x2, waiting for transfers between devices: 423 us -> 251 us  [local(): total = lax.psum(lax.psum(packed, 'sp'), 'dp')]
    all_to_all x1, waiting for transfers between devices: 24.2 us -> 0.01 us  [local(): lax.all_to_all(gated, 'sp', split_axis=0, concat_axis=1, tiled=True)]
    unnamed x4 -> x5, waiting for transfers between devices: 118 us -> 119 us
  transfers between devices with their start and end apart: 8 -> 9, of which waited for: 7 -> 7; matrix products, arithmetic and copies ran while one was open for 4% -> 6% of each run, Pallas kernels for 0% -> 0%
where the time goes in v1:
time: 635 us; the launch traced here: 634 us
  waiting for transfers between devices  485 us (76%)
  starting transfers between devices  46.6 us (7%)
  blocking collectives  37.3 us (6%)
  local copies, waits for them, and re-layouts  19.8 us (3%)
  matrix products  18.9 us (3%)
  between operations  13.9 us (2%)
  other arithmetic  12.7 us (2%)
    psum x2, waiting for transfers between devices, local(): total = lax.psum(lax.psum(packed, 'sp'), 'dp')  251 us
    unnamed x5, waiting for transfers between devices  119 us
    all_gather x1, waiting for transfers between devices, local(): weight_whole = lax.all_gather(weight_rows, 'dp', axis=0, tiled=True)  54.5 us
    all_gather x1, blocking collectives, local(): weight_rows = lax.all_gather(out_weight, 'sp', axis=1, tiled=True)  37.3 us
    all_to_all x1, waiting for transfers between devices, local(): lax.all_to_all(head_rows.astype(jnp.bfloat16), 'sp', split_axis=1, concat...  29.5 us
    all_to_all x2, waiting for transfers between devices, sum_over(): return lax.all_to_all(copies, axis, 0, 0, tiled=True).sum(axis=0)  17.5 us
    unnamed x18, local copies, waits for them, and re-layouts  15.4 us
    all_to_all x2, starting transfers between devices, sum_over(): return lax.all_to_all(copies, axis, 0, 0, tiled=True).sum(axis=0)  15 us
  transfers between devices with their start and end apart: 9, of which 7 were waited for; matrix products, arithmetic and copies ran while one was open for 6% of the time, Pallas kernels for 0%

profile of v1, /device:TPU:32, one launch (start us, length us, event | category | flops | bytes accessed | tf_op | source)
XLA Modules:
  0.0 634.0 jit_solution(1135314620933611738)
XLA Ops:
  7.2 0.0 copy-start
  7.2 0.0 all-gather.2.cloned.1.call-start
  7.2 37.3 %all_gather.6 = bf16[64,2048]{1,0:T(8,128)(2,1)} all-gather(bf16[64,128]{1,0:T(8,128)(2,1)} %param.11), channel_id=1, replica_groups=mesh['sp'=16,'dp'=32] {'sp'}, dimensions={1}, use_global_device_ids=true | all-gather | bytes 278528 | tf_op jit(solution)/shard_map/all_gather | solution.py:36
  44.6 0.0 all-gather.2.cloned.1.call-update
  44.6 1.8 fusion.58
  46.4 0.8 broadcast_in_dim.11
  47.2 8.9 %all-to-all-start.1 = ((f32[16,2,2048]{2,1,0:T(2,128)}), f32[16,2,2048]{2,1,0:T(2,128)S(1)}, u32[]{:S(2)}, u32[]{:S(2)}) async-start(f32[16,2,2048]{2,1,0:T(2,128)} %broadcast_in_dim.11), calls=%async_computation.1 | async-start | bytes 524288 | tf_op jit(solution)/shard_map/all_to_all | solution.py:17
  56.1 0.0 copy-start.2
  56.1 0.0 copy-start.1
  56.1 54.5 %all-gather.2.cloned.1.call-done = bf16[2048,2048]{1,0:T(8,128)(2,1)} async-done(((bf16[64,2048]{1,0:T(8,128)(2,1)}), bf16[2048,2048]{1,0:T(8,128)(2,1)}) %all-gather.2.cloned.1.call-update) | async-done | bytes 8388624 | tf_op jit(solution)/shard_map/all_gather | solution.py:37
  110.6 0.0 copy-done
  110.6 4.6 fusion.5
  115.3 0.0 copy-start.6
  115.3 0.9 copy.53
  116.2 0.0 all-to-all-done.1
  116.2 12.7 %all-to-all-start = ((bf16[128,16,128]{2,0,1:T(8,128)(2,1)}), bf16[128,16,128]{2,0,1:T(8,128)(2,1)S(1)}, u32[]{:S(2)}, u32[]{:S(2)}) async-start(bf16[128,16,128]{2,0,1:T(8,128)(2,1)} %bitcast.135), calls=%async_computation | async-start | bytes 1048576 | tf_op jit(solution)/shard_map/all_to_all | solution.py:61
  128.9 0.0 copy-done.5
  128.9 0.1 reduce_sum.92
  129.0 29.5 %all-to-all-done = bf16[128,16,128]{2,0,1:T(8,128)(2,1)S(1)} async-done(((bf16[128,16,128]{2,0,1:T(8,128)(2,1)}), bf16[128,16,128]{2,0,1:T(8,128)(2,1)S(1)}, u32[]{:S(2)}, u32[]{:S(2)}) %all-to-all-start) | async-done | bytes 524320 | tf_op jit(solution)/shard_map/all_to_all | solution.py:61
  158.6 0.0 copy-done.2
  158.6 0.5 fusion.59
  159.1 1.0 copy-done.3
  160.1 0.0 copy-done.1
  160.1 3.3 fusion.56
  163.4 0.8 broadcast_in_dim.15
  164.2 6.1 all-to-all-start.2
  170.3 0.0 copy-done.6
  170.3 0.7 fusion.80
  171.0 17.5 %all-to-all-done.2 = f32[16,2,2048]{2,1,0:T(2,128)S(1)} async-done(((f32[16,2,2048]{2,1,0:T(2,128)}), f32[16,2,2048]{2,1,0:T(2,128)S(1)}, u32[]{:S(2)}, u32[]{:S(2)}) %all-to-all-start.2) | async-done | bytes 262176 | tf_op jit(solution)/shard_map/all_to_all | solution.py:17
  188.6 0.1 reduce_sum.95
  188.7 2.8 fusion.51
  191.5 3.0 multiply_convert_fusion
  194.4 6.1 all-to-all-start.3
  200.5 0.0 all-reduce.3.cloned.1.call-start
  200.6 0.3 reduce_sum.99
  200.8 0.1 broadcast_bitcast_fusion
  200.9 2.5 fusion.6
  203.5 0.2 bitcast_multiply_fusion.5
  203.7 0.1 broadcast_multiply_fusion.2
  203.7 0.9 pad_maximum_fusion
  204.6 0.0 all-reduce.3.cloned.1.call-update
  204.6 0.0 all-reduce.5.cloned.1.call-start
  204.7 136.8 %all-reduce.3.cloned.1.call-done = f32[1064,128]{1,0:T(8,128)} async-done(((f32[1064,128]{1,0:T(8,128)}), f32[1064,128]{1,0:T(8,128)}) %all-reduce.3.cloned.1.call-update) | async-done | bytes 544784 | tf_op jit(solution)/shard_map/psum | solution.py:108
  341.5 0.0 all-reduce.5.cloned.1.call-update
  341.5 0.0 reduce-scatter.4.cloned.1.call-start
  341.5 0.0 all-to-all-done.3
  341.5 0.3 copy.36
  341.8 5.5 convert_bitcast_fusion
  347.4 12.3 %copy.42 = bf16[2048,2048]{1,0:T(8,128)(2,1)} copy(bf16[2048,2048]{0,1:T(8,128)(2,1)} %convert_bitcast_fusion) | data formatting | bytes 16777216
  359.7 0.0 reduce-scatter.4.cloned.1.call-update
  359.7 114.7 %all-reduce.5.cloned.1.call-done = f32[1064,128]{1,0:T(8,128)} async-done(((f32[1064,128]{1,0:T(8,128)}), f32[1064,128]{1,0:T(8,128)}) %all-reduce.5.cloned.1.call-update) | async-done | bytes 544784 | tf_op jit(solution)/shard_map/psum | solution.py:108
  474.4 0.7 slice.34
  475.1 119.4 %reduce-scatter.4.cloned.1.call-done = bf16[64,2048]{1,0:T(8,128)(2,1)} async-done(((bf16[2048,2048]{1,0:T(8,128)(2,1)}), bf16[64,2048]{1,0:T(8,128)(2,1)}) %reduce-scatter.4.cloned.1.call-update) | async-done | bytes 262160
  594.5 1.2 copy.43
  595.7 0.9 copy.37
  596.6 12.7 %all-to-all-start.4 = ((bf16[16,64,128]{2,1,0:T(8,128)(2,1)}), bf16[16,64,128]{2,1,0:T(8,128)(2,1)S(1)}, u32[]{:S(2)}, u32[]{:S(2)}) async-start(bf16[16,64,128]{2,1,0:T(8,128)(2,1)} %bitcast.29), calls=%async_computation.4 | async-start | bytes 524288 | tf_op jit(solution)/shard_map/all_to_all | solution.py:72
  609.3 0.5 fusion.84
  609.8 1.3 slice_multiply_fusion.5
  611.1 1.9 slice_multiply_fusion
  612.9 0.0 copy-done.4
  612.9 1.5 fusion.30
  614.4 12.1 %all-to-all-done.4 = bf16[16,64,128]{2,1,0:T(8,128)(2,1)S(1)} async-done(((bf16[16,64,128]{2,1,0:T(8,128)(2,1)}), bf16[16,64,128]{2,1,0:T(8,128)(2,1)S(1)}, u32[]{:S(2)}, u32[]{:S(2)}) %all-to-all-start.4) | async-done | bytes 262176 | tf_op jit(solution)/shard_map/all_to_all | solution.py:72
  626.6 0.1 copy.46
  626.7 0.7 copy.39
  (15 shorter events, 0.2 us)
Async XLA Ops:
  7.2 103.5 %copy-start = (bf16[1,128,2048]{2,1,0:T(8,128)(2,1)S(1)}, bf16[1,128,2048]{2,1,0:T(8,128)(2,1)}, u32[]{:S(2)}) copy-start(bf16[1,128,2048]{2,1,0:T(8,128)(2,1)} %param.8) | copy-start | bytes 1572868
  7.2 103.4 %all-gather.2.cloned.1.call-start = ((), (), s32[]{:S(2)}) async-start(), calls=%async_computation.6 | async-start | bytes 8650752 | tf_op jit(solution)/shard_map/all_gather | solution.py:37
  47.2 69.0 %all-to-all-start.1 = ((f32[16,2,2048]{2,1,0:T(2,128)}), f32[16,2,2048]{2,1,0:T(2,128)S(1)}, u32[]{:S(2)}, u32[]{:S(2)}) async-start(f32[16,2,2048]{2,1,0:T(2,128)} %broadcast_in_dim.11), calls=%async_computation.1 | async-start | bytes 524288 | tf_op jit(solution)/shard_map/all_to_all | solution.py:17
  56.1 72.8 %copy-start.5 = (bf16[128]{0:T(256)(128)(2,1)S(1)}, bf16[128]{0:T(256)(128)(2,1)}, u32[]{:S(2)}) copy-start(bf16[128]{0:T(256)(128)(2,1)} %param.14) | copy-start | bytes 772
  56.1 102.5 %copy-start.2 = (bf16[1,2048,128]{2,1,0:T(8,128)(2,1)S(1)}, bf16[1,2048,128]{2,1,0:T(8,128)(2,1)}, u32[]{:S(2)}) copy-start(bf16[1,2048,128]{2,1,0:T(8,128)(2,1)} %param.9) | copy-start | bytes 1572868
  56.1 104.0 %copy-start.1 = (bf16[1,2048,128]{2,1,0:T(8,128)(2,1)S(1)}, bf16[1,2048,128]{2,1,0:T(8,128)(2,1)}, u32[]{:S(2)}) copy-start(bf16[1,2048,128]{2,1,0:T(8,128)(2,1)} %param.10) | copy-start | bytes 1572868
  115.3 55.1 %copy-start.6 = (bf16[128]{0:T(256)(128)(2,1)S(1)}, bf16[128]{0:T(256)(128)(2,1)}, u32[]{:S(2)}) copy-start(bf16[128]{0:T(256)(128)(2,1)} %param.15) | copy-start | bytes 772
  116.2 42.4 %all-to-all-start = ((bf16[128,16,128]{2,0,1:T(8,128)(2,1)}), bf16[128,16,128]{2,0,1:T(8,128)(2,1)S(1)}, u32[]{:S(2)}, u32[]{:S(2)}) async-start(bf16[128,16,128]{2,0,1:T(8,128)(2,1)} %bitcast.135), calls=%async_computation | async-start | bytes 1048576 | tf_op jit(solution)/shard_map/all_to_all | solution.py:61
  159.1 1.0 copy-start.3
  164.2 24.4 %all-to-all-start.2 = ((f32[16,2,2048]{2,1,0:T(2,128)}), f32[16,2,2048]{2,1,0:T(2,128)S(1)}, u32[]{:S(2)}, u32[]{:S(2)}) async-start(f32[16,2,2048]{2,1,0:T(2,128)} %broadcast_in_dim.15), calls=%async_computation.2 | async-start | bytes 524288 | tf_op jit(solution)/shard_map/all_to_all | solution.py:17
  194.4 147.1 %all-to-all-start.3 = ((bf16[16,128,128]{2,1,0:T(8,128)(2,1)}), bf16[16,128,128]{2,1,0:T(8,128)(2,1)S(1)}, u32[]{:S(2)}, u32[]{:S(2)}) async-start(bf16[16,128,128]{2,1,0:T(8,128)(2,1)} %get-tuple-element.36), calls=%async_computation.3 | async-start | bytes 1048576 | tf_op jit(solution)/shard_map/all_to_all | solution.py:59
  200.5 141.0 %all-reduce.3.cloned.1.call-start = ((), (), s32[]{:S(2)}) async-start(), calls=%async_computation.7 | async-start | bytes 1089536 | tf_op jit(solution)/shard_map/psum | solution.py:108
  204.6 269.8 %all-reduce.5.cloned.1.call-start = ((), (), s32[]{:S(2)}) async-start(), calls=%async_computation.8 | async-start | bytes 1089536 | tf_op jit(solution)/shard_map/psum | solution.py:108
  341.5 253.0 %reduce-scatter.4.cloned.1.call-start = ((), (), s32[]{:S(2)}) async-start(), calls=%async_computation.9 | async-start | bytes 8650752
  359.7 253.2 %copy-start.4 = (f32[16,128,128]{2,1,0:T(8,128)S(1)}, f32[16,128,128]{2,1,0:T(8,128)}, u32[]{:S(2)}) copy-start(f32[16,128,128]{2,1,0:T(8,128)} %get-tuple-element.37) | copy-start | bytes 3145732
  596.6 30.0 %all-to-all-start.4 = ((bf16[16,64,128]{2,1,0:T(8,128)(2,1)}), bf16[16,64,128]{2,1,0:T(8,128)(2,1)S(1)}, u32[]{:S(2)}, u32[]{:S(2)}) async-start(bf16[16,64,128]{2,1,0:T(8,128)(2,1)} %bitcast.29), calls=%async_computation.4 | async-start | bytes 524288 | tf_op jit(solution)/shard_map/all_to_all | solution.py:72
Sparse Core Ops, SparseCore 0:
  44.7 65.8 all-gather.1
  204.7 136.6 all-reduce.2
  344.7 129.6 all-reduce.4
  478.8 115.5 reduce-scatter.3
